TPU v7x, 32 devices: a whole 2x2x4 slice. The times are simulated.
32 devices in a mesh: kv: 8 (over z, y), tp: 4 (over x, core).
Axes of the slice: x: 2, y: 2, z: 4, core: 2. Of those that a mesh axis runs over, the one named last changes fastest.
Arguments:
- tokens: bfloat16 [5120, 4096], P('kv'), may hold values from -48 to 48
- query_weight: bfloat16 [4096, 2048], P(None, 'tp'), may hold values from -0.09375 to 0.09375
- key_weight: bfloat16 [4096, 512], P(None, 'tp'), may hold values from -0.09375 to 0.09375
- value_weight: bfloat16 [4096, 512], P(None, 'tp'), may hold values from -0.09375 to 0.09375
- gate_weight: bfloat16 [4096, 64], replicated, may hold values from -0.09375 to 0.09375
- summary_pos: bfloat16 [32, 64], replicated, may hold values from -6 to 6
- key_mixing: bfloat16 [32, 8], replicated, may hold values from -1 to 1
- value_mixing: bfloat16 [32, 8], replicated, may hold values from -1 to 1
- out_weight: bfloat16 [2048, 4096], P('tp'), may hold values from -0.125 to 0.125
- chosen: int32 [80, 8, 16], P('kv', 'tp'), may hold values from 0 to 79, as said below
Outputs:
- mixed: bfloat16 [5120, 4096], P(('kv', 'tp'))
Inputs may be any that keep to these rules, and one draw needn't show every extreme that they name: `chosen`: entry [b, g, 0] is b itself; every entry is at most b. For the query blocks of one index of kv, one key head and any OTHER index of kv, at most 2 distinct blocks of that index's 64-position blocks are named, and exactly 2 of the index just before. Entries may repeat.
All inputs are finite; a program needn't handle non-finite values.
Results may differ from a plain program's by a relative error of at most 0.013.
The roundings to bfloat16 on the way count: a program that leaves them out, or rounds other values in their place, can miss the bound.
Values may be sent and summed in bfloat16 or wider, within the bound.
A program may use at most 192 MiB of HBM per device.

v0:
```python
import jax
import jax.numpy as jnp
from jax import lax
from jax.sharding import PartitionSpec as P

HD = 64
CMP = 32
SB = 64
N_SEL = 16


floor_score = -1e30


def masked_weights(scores, visible):
    probs = jax.nn.softmax(jnp.where(visible, scores, floor_score), axis=-1)
    return jnp.where(jnp.any(visible, axis=-1, keepdims=True), probs, 0.0)


def first_named(picked_ids):
    slot_count = picked_ids.shape[-1]
    repeated = picked_ids[..., :, None] == picked_ids[..., None, :]
    earlier = jnp.arange(slot_count)[None, :] < jnp.arange(slot_count)[:, None]
    return jnp.logical_not(jnp.any(repeated & earlier, axis=-1))


def summarize(source, offsets, mixing):
    span_count = source.shape[0] // CMP
    windows = source.astype(jnp.float32).reshape(span_count, CMP, source.shape[1], HD)
    windows = windows + offsets.astype(jnp.float32)[None, :, None, :]
    return jnp.einsum(
        "njgd,jg->ngd", windows, mixing.astype(jnp.float32), precision=lax.Precision.HIGHEST
    ).astype(jnp.bfloat16)


def local(
    tokens,
    query_weight,
    key_weight,
    value_weight,
    gate_weight,
    summary_pos,
    key_mixing,
    value_mixing,
    out_weight,
    chosen,
):
    tok_rows = tokens.shape[0]
    own_index = lax.axis_index("kv")
    head_part = lax.axis_index("tp")
    local_heads = query_weight.shape[1] // HD
    key_heads = key_weight.shape[1] // HD
    group_size = local_heads // key_heads
    own_blocks = tok_rows // SB
    score_scale = HD ** (-0.5)
    queries = jnp.dot(tokens, query_weight, preferred_element_type=jnp.float32).astype(jnp.bfloat16)
    queries = queries.reshape(tok_rows, key_heads, group_size, HD)
    key_rows = jnp.dot(tokens, key_weight, preferred_element_type=jnp.float32).astype(jnp.bfloat16)
    key_rows = key_rows.reshape(tok_rows, key_heads, HD)
    value_rows = jnp.dot(tokens, value_weight, preferred_element_type=jnp.float32).astype(
        jnp.bfloat16
    )
    value_rows = value_rows.reshape(tok_rows, key_heads, HD)
    gate_cols = lax.dynamic_slice_in_dim(
        gate_weight, head_part * local_heads * 2, local_heads * 2, 1
    )
    gate_vals = jax.nn.sigmoid(jnp.dot(tokens, gate_cols, preferred_element_type=jnp.float32))
    gate_vals = gate_vals.reshape(tok_rows, key_heads, group_size, 2)
    key_cols = lax.dynamic_slice_in_dim(key_mixing, head_part * key_heads, key_heads, 1)
    value_cols = lax.dynamic_slice_in_dim(value_mixing, head_part * key_heads, key_heads, 1)
    summary_pair = jnp.concatenate(
        [
            summarize(key_rows, summary_pos, key_cols),
            summarize(value_rows, summary_pos, value_cols),
        ],
        axis=-1,
    )
    summary_all = lax.all_gather(summary_pair, "kv", axis=0, tiled=True)
    span_ends = jnp.arange(summary_all.shape[0], dtype=jnp.int32) * CMP + (CMP - 1)
    query_pos = own_index * tok_rows + jnp.arange(tok_rows, dtype=jnp.int32)
    summary_scores = (
        jnp.einsum(
            "qgrd,ngd->grqn", queries, summary_all[..., :HD], preferred_element_type=jnp.float32
        )
        * score_scale
    )
    summary_probs = masked_weights(
        summary_scores, (span_ends[None, :] <= query_pos[:, None])[None, None]
    )
    summary_out = jnp.einsum(
        "grqn,ngd->qgrd",
        summary_probs.astype(jnp.bfloat16),
        summary_all[..., HD:],
        preferred_element_type=jnp.float32,
    )
    pair_rows = jnp.concatenate([key_rows, value_rows], axis=-1)
    head_ids = jnp.arange(key_heads, dtype=jnp.int32)[None, :, None]
    whole = lax.all_gather(pair_rows, "kv", axis=0, tiled=True)
    block_table = whole.reshape(-1, SB, key_heads, 2 * HD)
    picked = block_table[chosen, :, head_ids, :]
    picked = picked.reshape(own_blocks, key_heads, N_SEL * SB, 2 * HD)
    key_pos = (chosen[..., None] * SB + jnp.arange(SB, dtype=jnp.int32)).reshape(
        own_blocks, key_heads, N_SEL * SB
    )
    unique = first_named(chosen)
    counted = jnp.broadcast_to(unique[..., None], chosen.shape + (SB,)).reshape(
        own_blocks, key_heads, N_SEL * SB
    )
    block_pos = query_pos.reshape(own_blocks, SB)
    visible = counted[:, :, None, None, :] & (
        key_pos[:, :, None, None, :] <= block_pos[:, None, None, :, None]
    )
    query_blocks = queries.reshape(own_blocks, SB, key_heads, group_size, HD)
    chosen_scores = (
        jnp.einsum(
            "bqgrd,bgmd->bgrqm", query_blocks, picked[..., :HD], preferred_element_type=jnp.float32
        )
        * score_scale
    )
    chosen_probs = masked_weights(chosen_scores, visible)
    chosen_out = jnp.einsum(
        "bgrqm,bgmd->bqgrd",
        chosen_probs.astype(jnp.bfloat16),
        picked[..., HD:],
        preferred_element_type=jnp.float32,
    )
    chosen_out = chosen_out.reshape(tok_rows, key_heads, group_size, HD)
    blended = gate_vals[..., 0:1] * summary_out + gate_vals[..., 1:2] * chosen_out
    attention = blended.astype(jnp.bfloat16).reshape(tok_rows, local_heads * HD)
    return lax.psum_scatter(
        jnp.dot(attention, out_weight, preferred_element_type=jnp.float32).astype(jnp.bfloat16),
        "tp",
        scatter_dimension=0,
        tiled=True,
    )


def solution(mesh):
    placed = (
        P("kv", None),
        P(None, "tp"),
        P(None, "tp"),
        P(None, "tp"),
        P(),
        P(),
        P(),
        P(),
        P("tp", None),
        P("kv", "tp", None),
    )
    return jax.shard_map(
        local, mesh=mesh, in_specs=placed, out_specs=P(("kv", "tp"), None), check_vma=False
    )
```

profile of v0, /device:TPU:29, one launch (start us, length us, event | category | flops | bytes accessed | tf_op | source)
XLA Modules:
  0.0 200.3 jit_solution(13431939649227354241)
XLA Ops:
  6.5 1.2 copy-done
  7.8 4.3 %convolution_convert_fusion.3 = bf16[640,128]{0,1:T(8,128)(2,1)S(1)} fusion(bf16[640,4096]{1,0:T(8,128)(2,1)} %param.10, bf16[4096,128]{1,0:T(8,128)(2,1)S(1)} %copy-done), kind=kOutput, calls=%fused_computation.34 | convolution fusion | flops 671170560 | bytes 6455296 | tf_op jit(solution)/shard_map/dot_general | solution.py:58
  12.1 1.7 convolution_convert_fusion.2
  13.9 0.2 copy.47
  14.1 0.2 copy.46
  14.3 0.9 pad_maximum_fusion
  15.2 0.0 all-gather.2.cloned.1.call-update
  15.3 0.0 reduce-scatter.2.cloned.1.call-start
  15.3 0.1 copy.43
  15.5 0.1 copy.42
  15.6 0.5 and_reduce_fusion.1
  16.2 0.1 add.111
  16.3 0.1 reshape.164
  16.4 0.1 broadcast_in_dim.87
  16.5 0.1 and.35
  16.7 4.0 %fusion.23 = f32[640,16]{0,1:T(8,128)S(1)} fusion(bf16[640,4096]{1,0:T(8,128)(2,1)} %param.10, bf16[4096,64]{0,1:T(8,128)(2,1)} %param.14, s32[]{:T(128)S(6)} %select_n.27), kind=kOutput, calls=%fused_computation.39 | convolution fusion | flops 83916800 | bytes 5414916 | tf_op jit(solution)/shard_map/dot_general | solution.py:67
  20.8 0.1 add.108
  20.9 0.1 add.109
  21.0 0.4 reshape.163
  21.4 0.4 reshape.162
  21.8 0.7 fusion.48
  22.5 0.5 broadcast_add_fusion.1
  23.0 0.3 fusion.26
  23.4 0.3 fusion.24
  23.7 0.1 pad_maximum_fusion.1
  23.8 24.8 %all_gather.6 = bf16[160,2,128]{2,1,0:T(2,128)(2,1)S(1)} all-gather(bf16[20,2,128]{2,1,0:T(2,128)(2,1)S(1)} %pad_maximum_fusion.1), channel_id=1, replica_groups=mesh['kv'=8,'tp'=4] {'kv'}, dimensions={0}, use_global_device_ids=true | all-gather | bytes 92160 | tf_op jit(solution)/shard_map/all_gather | solution.py:78
  48.6 0.2 fusion.56
  48.7 0.1 copy.72
  48.8 0.1 copy.73
  48.9 7.2 %convolution_convert_fusion.1 = bf16[640,512]{0,1:T(8,128)(2,1)S(1)} fusion(bf16[640,4096]{1,0:T(8,128)(2,1)} %param.10, bf16[4096,512]{1,0:T(8,128)(2,1)} %param.11), kind=kOutput, calls=%fused_computation.31 | convolution fusion | flops 2684682240 | bytes 10092544 | tf_op jit(solution)/shard_map/dot_general | solution.py:56
  56.2 1.4 reshape.184
  57.6 0.1 compare_reduce_fusion
  57.8 1.0 and_reduce_fusion
  58.8 0.1 broadcast_compare_fusion
  58.9 3.0 %fusion.58 = (f32[2,4,640]{2,1,0:T(4,128)S(1)}, f32[2,4,640,160]{2,3,1,0:T(8,128)}) fusion(pred[640,160]{0,1:T(8,128)(4,1)S(1)} %broadcast_compare_fusion, bf16[640,2,4,64]{0,3,2,1:T(8,128)(2,1)S(1)} %bitcast.135, bf16[160,2,64]{0,2,1:T(8,128)(2,1)S(1)} %copy.73), kind=kOutput, calls=%fused_computation.89 | convolution fusion | flops 108134560 | bytes 4096000 | tf_op jit(solution)/shard_map/sub | solution.py:16
  61.9 2.2 %compare_and_fusion = pred[10,2,64,1024]{3,2,1,0:T(8,128)(4,1)} fusion(s32[10,64]{1,0:T(8,128)S(1)} %add_add_fusion, s32[10,2,1024]{2,1,0:T(2,128)S(1)} %broadcast_add_fusion.2, pred[10,2,1024]{2,1,0:T(4,128)(4,1)S(1)} %copy.51), kind=kLoop, calls=%fused_computation.15 | loop fusion | flops 2621440 | bytes 1415680 | tf_op jit(solution)/shard_map/and | solution.py:110
  64.1 4.3 %all-gather.2.cloned.1.call-done = bf16[5120,2,128]{2,0,1:T(8,128)(2,1)} async-done(((bf16[640,2,128]{2,0,1:T(8,128)(2,1)}), bf16[5120,2,128]{2,0,1:T(8,128)(2,1)}) %all-gather.2.cloned.1.call-update) | async-done | bytes 2621456 | tf_op jit(solution)/shard_map/all_gather | solution.py:98
  68.5 4.1 %copy.48 = bf16[80,64,2,128]{3,1,2,0:T(8,128)(2,1)} copy(bf16[80,64,2,128]{3,1,0,2:T(8,128)(2,1)} %bitcast.131) | data formatting | bytes 5242880 | tf_op jit(solution)/shard_map/reshape | solution.py:99
  72.5 6.8 %gather_fusion = bf16[320,64,128]{2,1,0:T(8,128)(2,1)} fusion(bf16[80,64,2,128]{3,1,2,0:T(8,128)(2,1)} %copy.48, s32[320]{0:T(512)S(1)} %reshape.164), kind=kCustom, calls=%fused_computation | custom fusion | bytes 10488320 | tf_op jit(solution)/shard_map/gather | solution.py:100
  79.4 11.2 %fusion.7 = f32[10,2,1024,64,4]{2,3,4,1,0:T(8,128)} fusion(bf16[10,2,1024,128]{3,2,1,0:T(8,128)(2,1)} %bitcast.126, bf16[10,64,2,4,64]{1,0,4,3,2:T(8,128)(2,1)S(1)} %reshape.184), kind=kOutput, calls=%fused_computation.13 | convolution fusion | flops 671088640 | bytes 26869760 | tf_op jit(solution)/shard_map/bqgrd,bgmd->bgrqm/dot_general | solution.py:115
  90.5 22.1 %fusion.63 = (f32[10,2,4,64]{3,2,1,0:T(4,128)S(1)}, f32[10,2,4,64,1024]{4,3,2,1,0:T(8,128)}) fusion(f32[10,2,1024,64,4]{2,3,4,1,0:T(8,128)} %fusion.7, pred[10,2,64,1024]{3,2,1,0:T(8,128)(4,1)} %compare_and_fusion), kind=kOutput, calls=%fused_computation.90 | output fusion | flops 31458304 | bytes 43274240 | tf_op jit(solution)/shard_map/sub | solution.py:16
  112.7 13.2 %fusion.9 = f32[10,64,2,4,64]{1,4,3,2,0:T(8,128)} fusion(f32[10,2,4,64,1024]{4,3,2,1,0:T(8,128)} %get-tuple-element.14, f32[10,2,4,64]{3,2,1,0:T(4,128)S(1)} %get-tuple-element.13, pred[10,2,64]{2,1,0:T(4,128)(4,1)S(1)} %and_reduce_fusion, bf16[10,2,1024,128]{3,2,1,0:T(8,128)(2,1)S(1)} %bitcast.129), kind=kOutput, calls=%fused_computation.21 | convolution fusion | flops 686817280 | bytes 27546880 | tf_op jit(solution)/shard_map/bgrqm,bgmd->bqgrd/dot_general | solution.py:121
  125.9 3.2 %copy.56 = f32[10,64,2,4,64]{4,1,0,3,2:T(8,128)} copy(f32[10,64,2,4,64]{1,4,3,2,0:T(8,128)} %fusion.9) | data formatting | bytes 2621440 | tf_op jit(solution)/shard_map/bgrqm,bgmd->bqgrd/transpose | solution.py:121
  129.1 2.1 %copy.57 = f32[640,2,4,64]{0,3,2,1:T(8,128)S(1)} copy(f32[640,2,4,64]{3,0,2,1:T(8,128)} %bitcast.130) | data formatting | bytes 2621440 | tf_op jit(solution)/shard_map/reshape | solution.py:127
  131.3 2.6 %fusion.18 = bf16[640,2,4,64]{0,3,2,1:T(8,128)(2,1)S(1)} fusion(f32[2,4,640,160]{2,3,1,0:T(8,128)} %get-tuple-element.12, f32[2,4,640]{2,1,0:T(4,128)S(1)} %get-tuple-element.11, pred[640]{0:T(1024)(128)(4,1)S(1)} %compare_reduce_fusion, f32[640,2,4,64]{0,3,2,1:T(8,128)S(1)} %copy.57, f32[640,2,4]{0,2,1:T(4,128)S(1)} %get-tuple-element.17, ...), kind=kOutput, calls=%fused_computation.30 | convolution fusion | flops 108625920 | bytes 5345920 | tf_op jit(solution)/shard_map/grqn,ngd->qgrd/dot_general | solution.py:90
  133.8 0.6 copy-done.3
  134.4 4.7 %convolution_convert_fusion = bf16[640,4096]{1,0:T(8,128)(2,1)} fusion(bf16[640,512]{0,1:T(8,128)(2,1)S(1)} %bitcast.134, bf16[512,4096]{1,0:T(8,128)(2,1)S(1)} %copy-done.3), kind=kOutput, calls=%fused_computation.11 | convolution fusion | flops 2686976000 | bytes 10092544 | tf_op jit(solution)/shard_map/dot_general | solution.py:131
  139.1 54.3 %reduce-scatter.2.cloned.1.call-done = bf16[160,4096]{1,0:T(8,128)(2,1)} async-done(((bf16[640,4096]{1,0:T(8,128)(2,1)}), bf16[160,4096]{1,0:T(8,128)(2,1)}) %reduce-scatter.2.cloned.1.call-update) | async-done | bytes 1310736 | tf_op jit(solution)/shard_map/reduce_scatter | solution.py:130
  (36 shorter events, 0.3 us)
Async XLA Ops:
  6.5 1.2 copy-start
  6.5 5.5 %copy-start.4 = (bf16[4096,128]{1,0:T(8,128)(2,1)S(1)}, bf16[4096,128]{1,0:T(8,128)(2,1)}, u32[]{:S(2)}) copy-start(bf16[4096,128]{1,0:T(8,128)(2,1)} %param.13) | copy-start | bytes 3145732
  6.5 61.9 %all-gather.2.cloned.1.call-start = ((), (), s32[]{:S(2)}) async-start(), calls=%async_computation.1 | async-start | bytes 2949120 | tf_op jit(solution)/shard_map/all_gather | solution.py:98
  7.8 4.3 %copy-start.2 = (bf16[640,4096]{1,0:T(8,128)(2,1)S(1)}, bf16[640,4096]{1,0:T(8,128)(2,1)}, u32[]{:S(2)}) copy-start(bf16[640,4096]{1,0:T(8,128)(2,1)} %param.10) | copy-start | bytes 15728644
  12.1 3.5 %copy-start.5 = (s32[10,2,16]{2,1,0:T(2,128)S(1)}, s32[10,2,16]{2,1,0:T(2,128)}, u32[]{:S(2)}) copy-start(s32[10,2,16]{2,1,0:T(2,128)} %param.19) | copy-start | bytes 3844
  12.1 4.3 %copy-start.6 = (bf16[32,64]{1,0:T(8,128)(2,1)S(1)}, bf16[32,64]{1,0:T(8,128)(2,1)}, u32[]{:S(2)}) copy-start(bf16[32,64]{1,0:T(8,128)(2,1)} %param.15) | copy-start | bytes 12292
  15.3 178.2 %reduce-scatter.2.cloned.1.call-start = ((), (), s32[]{:S(2)}) async-start(), calls=%async_computation.2 | async-start | bytes 6553600 | tf_op jit(solution)/shard_map/reduce_scatter | solution.py:130
  79.4 33.3 %slice-start = ((s8[5242880]{0:T(1024)(128)(4,1)}), s8[4194304]{0:T(1024)(128)(4,1)S(1)}, s32[]{:S(2)}) async-start(s8[5242880]{0:T(1024)(128)(4,1)} %bitcast.127), calls=%async_computation.3 | async-start | bytes 8388608
  90.5 22.2 %slice-start.1 = ((s8[5242880]{0:T(1024)(128)(4,1)}), s8[1048576]{0:T(1024)(128)(4,1)S(1)}, s32[]{:S(2)}) async-start(s8[5242880]{0:T(1024)(128)(4,1)} %bitcast.127), calls=%async_computation.4 | async-start | bytes 2097152
  131.2 3.2 %copy-start.3 = (bf16[512,4096]{1,0:T(8,128)(2,1)S(1)}, bf16[512,4096]{1,0:T(8,128)(2,1)}, u32[]{:S(2)}) copy-start(bf16[512,4096]{1,0:T(8,128)(2,1)} %param.18) | copy-start | bytes 12582916
  133.8 59.6 %copy-start.1 = (bf16[4096,128]{1,0:T(8,128)(2,1)S(1)}, bf16[4096,128]{1,0:T(8,128)(2,1)}, u32[]{:S(2)}) copy-start(bf16[4096,128]{1,0:T(8,128)(2,1)} %param.12) | copy-start | bytes 3145732
Sparse Core Ops, SparseCore 0:
  15.4 53.0 all-gather.1
  139.3 54.1 reduce-scatter.1
where the time goes:
time: 203 us; the launch traced here: 200 us
  waiting for transfers between devices  58.7 us (29%)
  matrix products  52.5 us (26%)
  other arithmetic  27.7 us (14%)
  blocking collectives  24.8 us (12%)
  local copies, waits for them, and re-layouts  22.8 us (11%)
  between operations  13.8 us (7%)
    reduce_scatter x1, waiting for transfers between devices, local(): lax.psum_scatter(jnp.dot(attention, out_weight, preferred_element_type=jn...  54.3 us
    all_gather x1, blocking collectives, local(): summary_all = lax.all_gather(summary_pair, 'kv', axis=0, tiled=True)  24.8 us
    sub x1, other arithmetic, masked_weights(): probs = jax.nn.softmax(jnp.where(visible, scores, floor_score), axis=-1)  22.1 us
    dot_general x1, matrix products, local(): jnp.einsum('bgrqm,bgmd->bqgrd', chosen_probs.astype(jnp.bfloat16), picked...  13.2 us
    dot_general x1, matrix products, local(): jnp.einsum('bqgrd,bgmd->bgrqm', query_blocks, picked[..., :HD], preferred...  11.2 us
    dot_general x1, matrix products, local(): jnp.dot(tokens, query_weight, preferred_element_type=jnp.float32)  7.24 us
    gather x1, local copies, waits for them, and re-layouts, local(): picked = block_table[chosen, :, head_ids, :]  6.85 us
    dot_general x1, matrix products, local(): jnp.dot(attention, out_weight, preferred_element_type=jnp.float32)  4.69 us
  transfers between devices with their start and end apart: 2, of which 2 were waited for; matrix products, arithmetic and copies ran while one was open for 12% of the time, Pallas kernels for 0%

commit v1 on v0

v1 whole, which is shorter than its diff:
```python
import functools

import jax
import jax.numpy as jnp
from jax import lax
from jax.experimental import pallas as pl
from jax.experimental.pallas import tpu as pltpu
from jax.sharding import PartitionSpec as P

HD = 64
CMP = 32
SB = 64
N_SEL = 16
LANES = 128
LOW = -1e30
F32 = jnp.float32
BF16 = jnp.bfloat16
MESH = pl.DeviceIdType.MESH
VMEM_LIMIT = 64_000_000


def first_named(picked_ids):
    slot_count = picked_ids.shape[-1]
    repeated = picked_ids[..., :, None] == picked_ids[..., None, :]
    earlier = jnp.arange(slot_count)[None, :] < jnp.arange(slot_count)[:, None]
    return jnp.logical_not(jnp.any(repeated & earlier, axis=-1))


def project_kernel(
    n, G, R, nb, kc, pad,
    tok_hbm, qw_hbm, kw_hbm, vw_hbm, gw_hbm, req_ref, mix_ref, pos_ref,
    qp_ref, gate_ref, tab_ref, sum_ref,
    tok, qw, kvw, gw, acc, gacc, tf, req_in, send, sum_send,
    sem_tok, sem_kw, sem_vw, sem_qw, sem_gw,
    req_s, req_r, blk_s, blk_r, sum_s, sum_r,
):
    me = lax.axis_index("kv")
    rows = nb * SB
    depth = tok.shape[1]
    chunks = depth // kc
    spans = rows // CMP
    kvd = G * HD

    def part(i):
        return pl.ds(i * kc, kc)

    def loads(i):
        return [
            pltpu.make_async_copy(tok_hbm.at[:, part(i)], tok.at[:, part(i)], sem_tok.at[i]),
            pltpu.make_async_copy(kw_hbm.at[part(i)], kvw.at[part(i), pl.ds(0, kvd)], sem_kw.at[i]),
            pltpu.make_async_copy(vw_hbm.at[part(i)], kvw.at[part(i), pl.ds(kvd, kvd)], sem_vw.at[i]),
        ]

    def late(i):
        return [
            pltpu.make_async_copy(qw_hbm.at[part(i)], qw.at[part(i)], sem_qw.at[i]),
            pltpu.make_async_copy(gw_hbm.at[part(i)], gw.at[part(i)], sem_gw.at[i]),
        ]

    for i in range(chunks):
        for c in loads(i):
            c.start()
    for i in range(chunks):
        for c in late(i):
            c.start()

    barrier = pltpu.get_barrier_semaphore()
    for i in range(1, n):
        pl.semaphore_signal(
            barrier, inc=1, device_id={"kv": lax.rem(me + i, n)}, device_id_type=MESH
        )
    pl.semaphore_wait(barrier, n - 1)

    def req_copy(i):
        return pltpu.make_async_remote_copy(
            src_ref=req_ref.at[lax.rem(me + n - i, n)], dst_ref=req_in.at[i],
            send_sem=req_s.at[i], recv_sem=req_r.at[i],
            device_id={"kv": lax.rem(me + n - i, n)}, device_id_type=MESH,
        )

    def blk_copy(i):
        return pltpu.make_async_remote_copy(
            src_ref=send.at[i],
            dst_ref=tab_ref.at[pl.ds(G * nb + me * G * 2, G * 2)],
            send_sem=blk_s.at[i], recv_sem=blk_r.at[i],
            device_id={"kv": lax.rem(me + i, n)}, device_id_type=MESH,
        )

    def blk_arrival(i):
        s = lax.rem(me + n - i, n)
        return pltpu.make_async_remote_copy(
            src_ref=send.at[i],
            dst_ref=tab_ref.at[pl.ds(G * nb + s * G * 2, G * 2)],
            send_sem=blk_s.at[i], recv_sem=blk_r.at[i],
            device_id={"kv": lax.rem(me + i, n)}, device_id_type=MESH,
        )

    def sum_copy(i):
        return pltpu.make_async_remote_copy(
            src_ref=sum_send, dst_ref=sum_ref.at[me],
            send_sem=sum_s.at[i], recv_sem=sum_r.at[i],
            device_id={"kv": lax.rem(me + i, n)}, device_id_type=MESH,
        )

    def sum_arrival(i):
        return pltpu.make_async_remote_copy(
            src_ref=sum_send, dst_ref=sum_ref.at[lax.rem(me + n - i, n)],
            send_sem=sum_s.at[i], recv_sem=sum_r.at[i],
            device_id={"kv": lax.rem(me + i, n)}, device_id_type=MESH,
        )

    for i in range(1, n):
        req_copy(i).start()

    acc[:, : 2 * kvd] = jnp.zeros((rows, 2 * kvd), F32)

    def kv_step(i, carry):
        for c in loads(i):
            c.wait()
        acc[:, : 2 * kvd] += jnp.dot(tok[:, part(i)], kvw[part(i), :], preferred_element_type=F32)
        return carry

    lax.fori_loop(0, chunks, kv_step, 0)
    lane = lax.broadcasted_iota(jnp.int32, (SB, LANES), 1)
    lower = lane < HD

    def table_step(b, carry):
        r0 = pl.ds(b * SB, SB)
        for pair in range(G // 2):
            keys = acc[r0, pair * LANES : (pair + 1) * LANES].astype(BF16).astype(F32)
            vals = acc[r0, kvd + pair * LANES : kvd + (pair + 1) * LANES].astype(BF16).astype(F32)
            first = jnp.where(lower, keys, pltpu.roll(vals, HD, 1))
            second = jnp.where(lower, pltpu.roll(keys, HD, 1), vals)
            for g, t in ((2 * pair, first), (2 * pair + 1, second)):
                tf[g, b] = t
                tab_ref[g * nb + b] = t.astype(BF16)
        return carry

    lax.fori_loop(0, nb, table_step, 0)
    for g in range(G):
        t = tf[g].reshape(spans, CMP, LANES)
        w = (t + pos_ref[...][None]) * mix_ref[g][None]
        s = jnp.sum(w, axis=1)
        s = jnp.concatenate([s, jnp.zeros((pad - spans, LANES), F32)], axis=0)
        sum_send[g] = s.astype(BF16)
        sum_ref[me, g] = s.astype(BF16)
    for i in range(1, n):
        sum_copy(i).start()
    for i in range(1, n):
        req_copy(i).wait_recv()

        @pl.when(me + i < n)
        def _():
            wanted = req_in[i]
            for k in range(G * 2):
                g = k // 2
                want = jnp.broadcast_to(wanted[k : k + 1], (SB, LANES))
                block = tf[g, 0]
                for b in range(1, nb):
                    block = jnp.where(want == b, tf[g, b], block)
                send[i, k] = block.astype(BF16)
            blk_copy(i).start()

    acc[...] = jnp.zeros_like(acc)
    gacc[...] = jnp.zeros_like(gacc)

    def q_step(i, carry):
        for c in late(i):
            c.wait()
        acc[...] += jnp.dot(tok[:, part(i)], qw[part(i), :], preferred_element_type=F32)
        gacc[...] += jnp.dot(tok[:, part(i)], gw[part(i), :], preferred_element_type=F32)
        return carry

    lax.fori_loop(0, chunks, q_step, 0)
    gate_ref[...] = jax.nn.sigmoid(gacc[...])

    def query_step(b, carry):
        r0 = pl.ds(b * SB, SB)
        for g in range(G):
            for pair in range(R // 2):
                at = (g * R // 2 + pair) * LANES
                t = acc[r0, at : at + LANES].astype(BF16).astype(F32) * (HD ** -0.5)
                even = jnp.where(lower, t, 0.0)
                odd = jnp.where(lower, pltpu.roll(t, HD, 1), 0.0)
                qp_ref[g, b, 2 * pair * SB : (2 * pair + 1) * SB, :] = even.astype(BF16)
                qp_ref[g, b, (2 * pair + 1) * SB : (2 * pair + 2) * SB, :] = odd.astype(BF16)
        return carry

    lax.fori_loop(0, nb, query_step, 0)
    for i in range(1, n):
        sum_arrival(i).wait_recv()
        sum_copy(i).wait_send()
        req_copy(i).wait_send()

        @pl.when(me + i < n)
        def _():
            blk_copy(i).wait_send()

        @pl.when(me - i >= 0)
        def _():
            blk_arrival(i).wait_recv()


def attend_kernel(
    n, G, R, nb, pad, spans, cw,
    idx_ref, qp_ref, gate_ref, tab_ref, sum_ref, bias_ref, ow_hbm,
    out_ref,
    ow, att, kbuf, mine, dsend, drecv, xsend, xrecv,
    sem_w, d_s, d_r, x_s, x_r,
):
    me = lax.axis_index("kv")
    tp = lax.axis_index("tp")
    core = lax.rem(tp, 2)
    side = tp // 2
    partner = side * 2 + 1 - core
    across = (1 - side) * 2 + core
    rows = nb * SB
    quarter = rows // 4
    half_blocks = nb // 2
    width = out_ref.shape[1]
    chunks = width // cw
    group_rows = R * SB

    load = pltpu.make_async_copy(ow_hbm, ow, sem_w)
    load.start()

    barrier = pltpu.get_barrier_semaphore()
    for peer in (partner, across):
        pl.semaphore_signal(barrier, inc=1, device_id={"tp": peer}, device_id_type=MESH)
    pl.semaphore_wait(barrier, 2)

    row = lax.broadcasted_iota(jnp.int32, (group_rows, LANES), 0) % SB
    lane = lax.broadcasted_iota(jnp.int32, (group_rows, LANES), 1)
    tri = jnp.where((lane < SB) & (lane > row), LOW, 0.0)
    span_lane = lax.broadcasted_iota(jnp.int32, (group_rows, n * pad), 1)
    span_in = span_lane % pad
    span_end = ((span_lane // pad) * spans + span_in) * CMP + (CMP - 1)
    span_row = lax.broadcasted_iota(jnp.int32, (group_rows, n * pad), 0) % SB
    low64 = lax.broadcasted_iota(jnp.int32, (SB, LANES), 1) < HD
    gate_lane = lax.broadcasted_iota(jnp.int32, (SB, gate_ref.shape[1]), 1)
    nt = (((1,), (1,)), ((), ()))

    def attend(b, carry):
        gates = gate_ref[pl.ds(b * SB, SB), :]
        seen = (span_in < spans) & (span_end - span_row <= me * rows + b * SB)
        for g in range(G):
            base = (b * G + g) * N_SEL
            for j in range(N_SEL):
                kbuf[g, j * SB : (j + 1) * SB, :] = tab_ref[idx_ref[base + j]]
            kb = kbuf[g]
            q = qp_ref[g, b]
            s = lax.dot_general(q, kb, nt, preferred_element_type=F32)
            s = s + bias_ref[b * G + g]
            s = jnp.concatenate([s[:, :LANES] + tri, s[:, LANES:]], axis=1)
            m = jnp.max(s, axis=-1, keepdims=True)
            p = jnp.exp(s - m)
            l = jnp.sum(p, axis=-1, keepdims=True)
            oc = jnp.dot(p.astype(BF16), kb, preferred_element_type=F32)
            sm = sum_ref[:, g].reshape(n * pad, LANES)
            s2 = lax.dot_general(q, sm, nt, preferred_element_type=F32)
            s2 = jnp.where(seen, s2, LOW)
            m2 = jnp.max(s2, axis=-1, keepdims=True)
            p2 = jnp.where(seen, jnp.exp(s2 - m2), 0.0)
            l2 = jnp.sum(p2, axis=-1, keepdims=True)
            os = jnp.dot(p2.astype(BF16), sm, preferred_element_type=F32)
            ic = 1.0 / l
            i2 = jnp.where(l2 > 0.0, 1.0 / jnp.where(l2 > 0.0, l2, 1.0), 0.0)
            parts = []
            for r in range(R):
                at = (tp * G * R + g * R + r) * 2
                g0 = jnp.sum(jnp.where(gate_lane == at, gates, 0.0), axis=-1, keepdims=True)
                g1 = jnp.sum(jnp.where(gate_lane == at + 1, gates, 0.0), axis=-1, keepdims=True)
                k = slice(r * SB, (r + 1) * SB)
                parts.append(os[k] * (g0 * i2[k]) + oc[k] * (g1 * ic[k]))
            for pair in range(R // 2):
                t = jnp.where(low64, pltpu.roll(parts[2 * pair], HD, 1), parts[2 * pair + 1])
                at = (g * R // 2 + pair) * LANES
                att[pl.ds(b * SB, SB), at : at + LANES] = t.astype(BF16)
        return carry

    def d_copy(h, j):
        return pltpu.make_async_remote_copy(
            src_ref=dsend.at[h, j], dst_ref=drecv.at[h, j],
            send_sem=d_s.at[h, j], recv_sem=d_r.at[h, j],
            device_id={"tp": partner}, device_id_type=MESH,
        )

    def x_copy(j):
        return pltpu.make_async_remote_copy(
            src_ref=xsend.at[j], dst_ref=xrecv.at[j],
            send_sem=x_s.at[j], recv_sem=x_r.at[j],
            device_id={"tp": across}, device_id_type=MESH,
        )

    def product(h, first_row, j):
        cols = pl.ds(pl.multiple_of(j * cw, cw), cw)
        w = ow[:, cols]
        theirs = att[pl.ds(first_row + (1 - core) * quarter, quarter), :]
        dsend[h, j] = jnp.dot(theirs, w, preferred_element_type=F32).astype(BF16)
        d_copy(h, j).start()
        ours = att[pl.ds(first_row + core * quarter, quarter), :]
        mine[h, j] = jnp.dot(ours, w, preferred_element_type=F32).astype(BF16)

    def forward(j):
        d_copy(0, j).wait_recv()
        xsend[j] = (mine[0, j].astype(F32) + drecv[0, j].astype(F32)).astype(BF16)
        x_copy(j).start()

    other_first = (1 - side) * half_blocks
    lax.fori_loop(other_first, other_first + half_blocks, attend, 0)
    load.wait()
    product(0, other_first * SB, 0)

    def first_step(j, carry):
        product(0, other_first * SB, j)
        forward(j - 1)
        return carry

    lax.fori_loop(1, chunks, first_step, 0)
    forward(chunks - 1)

    own_first = side * half_blocks
    lax.fori_loop(own_first, own_first + half_blocks, attend, 0)

    def second_step(j, carry):
        product(1, own_first * SB, j)
        return carry

    lax.fori_loop(0, chunks, second_step, 0)

    def last_step(j, carry):
        cols = pl.ds(pl.multiple_of(j * cw, cw), cw)
        d_copy(1, j).wait_recv()
        x_copy(j).wait_recv()
        total = mine[1, j].astype(F32) + drecv[1, j].astype(F32) + xrecv[j].astype(F32)
        out_ref[:, cols] = total.astype(BF16)
        d_copy(0, j).wait_send()
        d_copy(1, j).wait_send()
        x_copy(j).wait_send()
        return carry

    lax.fori_loop(0, chunks, last_step, 0)


def local(
    n,
    tokens, query_weight, key_weight, value_weight, gate_weight,
    summary_pos, key_mixing, value_mixing, out_weight, chosen,
):
    rows, depth = tokens.shape
    me = lax.axis_index("kv")
    tp = lax.axis_index("tp")
    heads = query_weight.shape[1] // HD
    G = key_weight.shape[1] // HD
    R = heads // G
    nb = rows // SB
    spans = rows // CMP
    pad = -(-spans // 16) * 16
    kc = min(1024, depth)
    chunks = depth // kc
    width = out_weight.shape[1]
    cw = 512
    oc = width // cw
    gates_all = gate_weight.shape[1]

    source = chosen // nb
    inside = chosen - source * nb
    hit = source[None] == jnp.arange(n, dtype=jnp.int32)[:, None, None, None]
    lo = jnp.min(jnp.where(hit, inside[None], nb), axis=(1, 3))
    hi = jnp.max(jnp.where(hit, inside[None], -1), axis=(1, 3))
    lo = jnp.where(lo == nb, 0, lo)
    hi = jnp.where(hi < 0, 0, hi)
    req = jnp.stack([lo, hi], axis=-1).reshape(n, G * 2)
    req = jnp.pad(req, ((0, 0), (0, 8 - G * 2)))
    req = jnp.broadcast_to(req[:, :, None], (n, 8, LANES))
    low_of = jnp.sum(jnp.where(hit, lo[:, None, :, None], 0), axis=0)
    head = jnp.arange(G, dtype=jnp.int32)[None, :, None]
    away = G * nb + (source * G + head) * 2 + (inside != low_of).astype(jnp.int32)
    index = jnp.where(source == me, head * nb + inside, away).reshape(-1)
    bias = jnp.where(first_named(chosen), 0.0, LOW)
    bias = jnp.broadcast_to(bias[..., None], (nb, G, N_SEL, SB)).reshape(nb * G, 1, N_SEL * SB)

    km = lax.dynamic_slice_in_dim(key_mixing, tp * G, G, 1).astype(F32).T
    vm = lax.dynamic_slice_in_dim(value_mixing, tp * G, G, 1).astype(F32).T
    mix = jnp.concatenate(
        [
            jnp.broadcast_to(km[:, :, None], (G, CMP, HD)),
            jnp.broadcast_to(vm[:, :, None], (G, CMP, HD)),
        ],
        axis=-1,
    )
    pos = jnp.concatenate([summary_pos, summary_pos], axis=-1).astype(F32)

    vmem = pl.BlockSpec(memory_space=pltpu.VMEM)
    hbm = pl.BlockSpec(memory_space=pl.ANY)
    smem = pl.BlockSpec(memory_space=pltpu.SMEM)
    dma = pltpu.SemaphoreType.DMA
    table = G * nb + n * G * 2
    queries, gates, tab, summary = pl.pallas_call(
        functools.partial(project_kernel, n, G, R, nb, kc, pad),
        name="project",
        out_shape=[
            jax.ShapeDtypeStruct((G, nb, R * SB, LANES), BF16),
            jax.ShapeDtypeStruct((rows, gates_all), F32),
            jax.ShapeDtypeStruct((table, SB, LANES), BF16),
            jax.ShapeDtypeStruct((n, G, pad, LANES), BF16),
        ],
        in_specs=[hbm] * 5 + [vmem] * 3,
        out_specs=[vmem] * 4,
        scratch_shapes=[
            pltpu.VMEM((rows, depth), BF16),
            pltpu.VMEM((depth, heads * HD), BF16),
            pltpu.VMEM((depth, 2 * G * HD), BF16),
            pltpu.VMEM((depth, gates_all), BF16),
            pltpu.VMEM((rows, heads * HD), F32),
            pltpu.VMEM((rows, gates_all), F32),
            pltpu.VMEM((G, nb, SB, LANES), F32),
            pltpu.VMEM((n, 8, LANES), jnp.int32),
            pltpu.VMEM((n, G * 2, SB, LANES), BF16),
            pltpu.VMEM((G, pad, LANES), BF16),
            dma((chunks,)), dma((chunks,)), dma((chunks,)), dma((chunks,)), dma((chunks,)),
            dma((n,)), dma((n,)), dma((n,)), dma((n,)), dma((n,)), dma((n,)),
        ],
        compiler_params=pltpu.CompilerParams(
            collective_id=1, has_side_effects=True, vmem_limit_bytes=VMEM_LIMIT
        ),
    )(tokens, query_weight, key_weight, value_weight, gate_weight, req, mix, pos)

    quarter = rows // 4
    return pl.pallas_call(
        functools.partial(attend_kernel, n, G, R, nb, pad, spans, cw),
        name="attend",
        out_shape=jax.ShapeDtypeStruct((quarter, width), BF16),
        in_specs=[smem] + [vmem] * 5 + [hbm],
        out_specs=vmem,
        scratch_shapes=[
            pltpu.VMEM(out_weight.shape, BF16),
            pltpu.VMEM((rows, heads * HD), BF16),
            pltpu.VMEM((G, N_SEL * SB, LANES), BF16),
            pltpu.VMEM((2, oc, quarter, cw), BF16),
            pltpu.VMEM((2, oc, quarter, cw), BF16),
            pltpu.VMEM((2, oc, quarter, cw), BF16),
            pltpu.VMEM((oc, quarter, cw), BF16),
            pltpu.VMEM((oc, quarter, cw), BF16),
            dma, dma((2, oc)), dma((2, oc)), dma((oc,)), dma((oc,)),
        ],
        compiler_params=pltpu.CompilerParams(
            collective_id=2, has_side_effects=True, vmem_limit_bytes=VMEM_LIMIT
        ),
    )(index, queries, gates, tab, summary, bias, out_weight)


def solution(mesh):
    placed = (
        P("kv", None),
        P(None, "tp"),
        P(None, "tp"),
        P(None, "tp"),
        P(),
        P(),
        P(),
        P(),
        P("tp", None),
        P("kv", "tp", None),
    )
    return jax.shard_map(
        functools.partial(local, mesh.shape["kv"]),
        mesh=mesh, in_specs=placed, out_specs=P(("kv", "tp"), None), check_vma=False,
    )
```

time: 203 us -> 83.3 us (0.41)
  Pallas kernels: 0 us -> 69.2 us
  waiting for transfers between devices: 58.7 us -> 0 us
  matrix products: 52.5 us -> 0 us
  blocking collectives: 24.8 us -> 0 us
  other arithmetic: 27.7 us -> 5.96 us
  local copies, waits for them, and re-layouts: 22.8 us -> 7.31 us
  between operations: 13.8 us -> 0.08 us
    pallas_call x0 -> x2, Pallas kernels: none -> 69.2 us  [the longest x1 46.1 us: local(): pl.pallas_call(functools.partial(attend_kernel, n, G, R, nb, pad, spans,...]
    reduce_scatter x1 -> x0, waiting for transfers between devices: 54.3 us -> none  [local(): lax.psum_scatter(jnp.dot(attention, out_weight, preferred_element_type=jn...]
    dot_general x10 -> x0, matrix products: 49.6 us -> none  [the longest x1 13.2 us: local(): jnp.einsum('bgrqm,bgmd->bqgrd', chosen_probs.astype(jnp.bfloat16), picked...]
    all_gather x1 -> x0, blocking collectives: 24.8 us -> none  [local(): summary_all = lax.all_gather(summary_pair, 'kv', axis=0, tiled=True)]
    sub x1, other arithmetic: 22.1 us -> 0.74 us  [local(): inside = chosen - source * nb]
    gather x1 -> x0, local copies, waits for them, and re-layouts: 6.85 us -> none  [local(): picked = block_table[chosen, :, head_ids, :]]
    reshape x5 -> x2, local copies, waits for them, and re-layouts: 6.65 us -> 1.46 us  [the longest x1 0.78 us: local(): jnp.broadcast_to(bias[..., None], (nb, G, N_SEL, SB))]
    all_gather x1 -> x0, waiting for transfers between devices: 4.34 us -> none  [local(): whole = lax.all_gather(pair_rows, 'kv', axis=0, tiled=True)]
  transfers between devices with their start and end apart: 2 -> 0, of which waited for: 2 -> 0; matrix products, arithmetic and copies ran while one was open for 12% -> 0% of each run, Pallas kernels for 0% -> 0%
where the time goes in v1:
time: 83.3 us; the launch traced here: 82.5 us
  Pallas kernels  69.2 us (83%)
  local copies, waits for them, and re-layouts  7.31 us (9%)
  other arithmetic  5.96 us (7%)
    pallas_call x1, Pallas kernels, local(): pl.pallas_call(functools.partial(attend_kernel, n, G, R, nb, pad, spans,...  46.1 us
    pallas_call x1, Pallas kernels, local(): pl.pallas_call(functools.partial(project_kernel, n, G, R, nb, kc, pad), n...  23.1 us
    unnamed x3, local copies, waits for them, and re-layouts  4.93 us

profile of v1, /device:TPU:29, one launch (start us, length us, event | category | flops | bytes accessed | tf_op | source)
XLA Modules:
  0.0 82.5 jit_solution(8340378388237208819)
XLA Ops:
  0.0 0.7 convert_bitcast_fusion
  0.7 1.3 %and_reduce_fusion = pred[10,2,16]{2,1,0:T(4,128)(4,1)S(1)} fusion(s32[10,2,16]{2,1,0:T(2,128)} %param.19, pred[16,16]{1,0:T(8,128)(4,1)S(1)} %iota_compare_fusion.1), kind=kLoop, calls=%fused_computation | loop fusion | flops 15040 | bytes 1856 | tf_op jit(solution)/shard_map/reduce_or | solution.py:26
  2.0 1.5 %maximum_convert_fusion.pos_ref = f32[32,128]{1,0:T(8,128)} fusion(bf16[32,64]{1,0:T(8,128)(2,1)} %param.15), kind=kLoop, calls=%fused_computation.11 | loop fusion | flops 16384 | bytes 20480 | tf_op jit(solution)/shard_map/convert_element_type | solution.py:392
  3.5 0.7 multiply_subtract_fusion
  4.2 0.2 select_reduce_fusion
  4.4 0.1 copy.18
  4.5 0.1 select_reduce_fusion.1
  4.6 0.8 compare_select_fusion
  5.4 0.7 reshape.60.idx_ref
  6.1 0.7 broadcast_in_dim.87.req_ref
  6.8 0.1 broadcast_in_dim.89
  6.8 0.1 broadcast_in_dim.88
  6.9 0.7 pad_maximum_fusion.mix_ref
  7.6 0.1 broadcast_in_dim.92
  7.7 0.8 reshape.62.bias_ref
  8.5 2.4 %copy.17.gw_hbm = bf16[4096,64]{1,0:T(8,128)(2,1)} copy(bf16[4096,64]{0,1:T(8,128)(2,1)} %param.14) | data formatting | bytes 1048576 | tf_op args[4]
  10.8 23.1 %project.1 = (bf16[2,10,256,128]{3,2,1,0:T(8,128)(2,1)}, f32[640,64]{1,0:T(8,128)}, bf16[52,64,128]{2,1,0:T(8,128)(2,1)}, bf16[8,2,32,128]{3,2,1,0:T(8,128)(2,1)}) custom-call(bf16[640,4096]{1,0:T(8,128)(2,1)} %tok_hbm.1, bf16[4096,512]{1,0:T(8,128)(2,1)} %qw_hbm.1, bf16[4096,128]{1,0:T(8,128)(2,1)} %kw_hbm.1, bf16[4096,128]{1,0:T(8,128)(2,1)} %vw_hbm.1, ...), custom_call_target="tpu_custom_call" | custom-call | tf_op jit(solution)/shard_map/project/pallas_call | solution.py:399
  33.9 46.1 %attend.1 = bf16[160,4096]{1,0:T(8,128)(2,1)} custom-call(s32[320]{0:T(512)} %reshape.60.idx_ref, bf16[2,10,256,128]{3,2,1,0:T(8,128)(2,1)} %get-tuple-element.9.qp_ref, f32[640,64]{1,0:T(8,128)} %get-tuple-element.10.gate_ref, bf16[52,64,128]{2,1,0:T(8,128)(2,1)} %get-tuple-element.11.tab_ref, bf16[8,2,32,128]{3,2,1,0:T(8,128)(2,1)} %get-tuple-element.12.sum_ref, ...), custom_call_target="tpu_custom_call" | custom-call | tf_op jit(solution)/shard_map/attend/pallas_call | solution.py:430
  80.0 2.5 %copy.20 = bf16[160,4096]{1,0:T(8,128)(2,1)} copy(bf16[160,4096]{1,0:T(8,128)(2,1)} %attend.1) | data formatting | bytes 2621440
  (8 shorter events, 0.0 us)

commit v2 on v1

--- a/solution.py
+++ b/solution.py
@@ -19,18 +19,11 @@
 VMEM_LIMIT = 64_000_000
 
 
-def first_named(picked_ids):
-    slot_count = picked_ids.shape[-1]
-    repeated = picked_ids[..., :, None] == picked_ids[..., None, :]
-    earlier = jnp.arange(slot_count)[None, :] < jnp.arange(slot_count)[:, None]
-    return jnp.logical_not(jnp.any(repeated & earlier, axis=-1))
-
-
 def project_kernel(
     n, G, R, nb, kc, pad,
-    tok_hbm, qw_hbm, kw_hbm, vw_hbm, gw_hbm, req_ref, mix_ref, pos_ref,
-    qp_ref, gate_ref, tab_ref, sum_ref,
-    tok, qw, kvw, gw, acc, gacc, tf, req_in, send, sum_send,
+    tok_hbm, qw_hbm, kw_hbm, vw_hbm, gw_hbm, ch_ref, km_ref, vm_ref, pos_in,
+    qp_ref, gate_ref, tab_ref, sum_ref, idx_ref, bias_ref,
+    tok, qw, kvw, gw, acc, gacc, tf, named, pos_ref, req_ref, req_in, send, sum_send,
     sem_tok, sem_kw, sem_vw, sem_qw, sem_gw,
     req_s, req_r, blk_s, blk_r, sum_s, sum_r,
 ):
@@ -54,7 +47,7 @@
     def late(i):
         return [
             pltpu.make_async_copy(qw_hbm.at[part(i)], qw.at[part(i)], sem_qw.at[i]),
-            pltpu.make_async_copy(gw_hbm.at[part(i)], gw.at[part(i)], sem_gw.at[i]),
+            pltpu.make_async_copy(gw_hbm.at[:, part(i)], gw.at[:, part(i)], sem_gw.at[i]),
         ]
 
     for i in range(chunks):
@@ -69,6 +62,38 @@
         pl.semaphore_signal(
             barrier, inc=1, device_id={"kv": lax.rem(me + i, n)}, device_id_type=MESH
         )
+
+    place = lax.broadcasted_iota(jnp.int32, named.shape, 1)
+    slot_row = lax.broadcasted_iota(jnp.int32, (LANES, N_SEL * SB), 0)
+    slot_col = lax.broadcasted_iota(jnp.int32, (LANES, N_SEL * SB), 1) // SB
+    spread = jnp.where(slot_row == slot_col, 1.0, 0.0).astype(BF16)
+    for g in range(G):
+        named[...] = jnp.full(named.shape, -1.0, F32)
+        named[:nb, :N_SEL] = ch_ref[:, g, :].astype(F32)
+        c = named[...]
+        source = jnp.zeros_like(c)
+        for s in range(1, n):
+            source = source + jnp.where(c >= s * nb, 1.0, 0.0)
+        inside = c - source * nb
+        low_of = jnp.zeros_like(c)
+        for s in range(n):
+            hit = (c >= 0.0) & (source == s)
+            lo = jnp.where(hit, inside, float(nb))
+            lo = jnp.min(jnp.min(lo, axis=0, keepdims=True), axis=1, keepdims=True)
+            lo = jnp.where(lo == nb, 0.0, lo)
+            hi = jnp.where(hit, inside, 0.0)
+            hi = jnp.max(jnp.max(hi, axis=0, keepdims=True), axis=1, keepdims=True)
+            low_of = jnp.where(hit, lo, low_of)
+            req_ref[s, 2 * g : 2 * g + 1] = jnp.broadcast_to(lo, (1, LANES))
+            req_ref[s, 2 * g + 1 : 2 * g + 2] = jnp.broadcast_to(hi, (1, LANES))
+        away = G * nb + (source * G + g) * 2 + jnp.where(inside != low_of, 1.0, 0.0)
+        at = jnp.where(source == me.astype(F32), g * nb + inside, away)
+        idx_ref[g] = at[:nb, :N_SEL].astype(jnp.int32)
+        again = jnp.zeros_like(c)
+        for d in range(1, N_SEL):
+            again = jnp.where((place >= d) & (pltpu.roll(c, d, 1) == c), 1.0, again)
+        bias_ref[g] = jnp.dot(again.astype(BF16), spread, preferred_element_type=F32) * LOW
+
     pl.semaphore_wait(barrier, n - 1)
 
     def req_copy(i):
@@ -137,9 +162,26 @@
         return carry
 
     lax.fori_loop(0, nb, table_step, 0)
+    pos_ref[:, :HD] = pos_in[...].astype(F32)
+    pos_ref[:, HD:] = pos_in[...].astype(F32)
+    mix_row = lax.broadcasted_iota(jnp.int32, km_ref.shape, 0)
+    mix_low = lax.broadcasted_iota(jnp.int32, (CMP, LANES), 1) < HD
+    diagonal = lax.broadcasted_iota(jnp.int32, (CMP, CMP), 0) == lax.broadcasted_iota(
+        jnp.int32, (CMP, CMP), 1
+    )
+
+    def mix_column(ref, head):
+        line = jnp.where(mix_row == head, ref[...].astype(F32), 0.0)
+        line = jnp.sum(line, axis=0, keepdims=True)
+        return jnp.sum(jnp.where(diagonal, line, 0.0), axis=1, keepdims=True)
+
     for g in range(G):
+        head = lax.axis_index("tp") * G + g
+        km = mix_column(km_ref, head)
+        vm = mix_column(vm_ref, head)
+        mix = jnp.where(mix_low, km, vm)
         t = tf[g].reshape(spans, CMP, LANES)
-        w = (t + pos_ref[...][None]) * mix_ref[g][None]
+        w = (t + pos_ref[...][None]) * mix[None]
         s = jnp.sum(w, axis=1)
         s = jnp.concatenate([s, jnp.zeros((pad - spans, LANES), F32)], axis=0)
         sum_send[g] = s.astype(BF16)
@@ -157,7 +199,7 @@
                 want = jnp.broadcast_to(wanted[k : k + 1], (SB, LANES))
                 block = tf[g, 0]
                 for b in range(1, nb):
-                    block = jnp.where(want == b, tf[g, b], block)
+                    block = jnp.where(want == float(b), tf[g, b], block)
                 send[i, k] = block.astype(BF16)
             blk_copy(i).start()
 
@@ -168,7 +210,9 @@
         for c in late(i):
             c.wait()
         acc[...] += jnp.dot(tok[:, part(i)], qw[part(i), :], preferred_element_type=F32)
-        gacc[...] += jnp.dot(tok[:, part(i)], gw[part(i), :], preferred_element_type=F32)
+        gacc[...] += lax.dot_general(
+            tok[:, part(i)], gw[:, part(i)], (((1,), (1,)), ((), ())), preferred_element_type=F32
+        )
         return carry
 
     lax.fori_loop(0, chunks, q_step, 0)
@@ -205,29 +249,30 @@
     n, G, R, nb, pad, spans, cw,
     idx_ref, qp_ref, gate_ref, tab_ref, sum_ref, bias_ref, ow_hbm,
     out_ref,
-    ow, att, kbuf, mine, dsend, drecv, xsend, xrecv,
-    sem_w, d_s, d_r, x_s, x_r,
+    ow, att, kbuf, mine, dsend, drecv, early, esend, erecv, xsend, xrecv, base,
+    sem_w, d_s, d_r, e_s, e_r, x_s, x_r,
 ):
     me = lax.axis_index("kv")
     tp = lax.axis_index("tp")
     core = lax.rem(tp, 2)
     side = tp // 2
     partner = side * 2 + 1 - core
-    across = (1 - side) * 2 + core
     rows = nb * SB
     quarter = rows // 4
     half_blocks = nb // 2
     width = out_ref.shape[1]
     chunks = width // cw
     group_rows = R * SB
+    side_cols = width // 2
+    step_rows = SB // 2
 
     load = pltpu.make_async_copy(ow_hbm, ow, sem_w)
     load.start()
 
     barrier = pltpu.get_barrier_semaphore()
-    for peer in (partner, across):
-        pl.semaphore_signal(barrier, inc=1, device_id={"tp": peer}, device_id_type=MESH)
-    pl.semaphore_wait(barrier, 2)
+    for i in range(1, 4):
+        pl.semaphore_signal(barrier, inc=1, device_id={"tp": lax.rem(tp + i, 4)}, device_id_type=MESH)
+    pl.semaphore_wait(barrier, 3)
 
     row = lax.broadcasted_iota(jnp.int32, (group_rows, LANES), 0) % SB
     lane = lax.broadcasted_iota(jnp.int32, (group_rows, LANES), 1)
@@ -244,13 +289,12 @@
         gates = gate_ref[pl.ds(b * SB, SB), :]
         seen = (span_in < spans) & (span_end - span_row <= me * rows + b * SB)
         for g in range(G):
-            base = (b * G + g) * N_SEL
             for j in range(N_SEL):
-                kbuf[g, j * SB : (j + 1) * SB, :] = tab_ref[idx_ref[base + j]]
+                kbuf[g, j * SB : (j + 1) * SB, :] = tab_ref[idx_ref[g, b, j]]
             kb = kbuf[g]
             q = qp_ref[g, b]
             s = lax.dot_general(q, kb, nt, preferred_element_type=F32)
-            s = s + bias_ref[b * G + g]
+            s = s + bias_ref[g, pl.ds(b, 1), :]
             s = jnp.concatenate([s[:, :LANES] + tri, s[:, LANES:]], axis=1)
             m = jnp.max(s, axis=-1, keepdims=True)
             p = jnp.exp(s - m)
@@ -278,68 +322,103 @@
                 att[pl.ds(b * SB, SB), at : at + LANES] = t.astype(BF16)
         return carry
 
-    def d_copy(h, j):
-        return pltpu.make_async_remote_copy(
-            src_ref=dsend.at[h, j], dst_ref=drecv.at[h, j],
-            send_sem=d_s.at[h, j], recv_sem=d_r.at[h, j],
+    def d_copy(j):
+        return pltpu.make_async_remote_copy(
+            src_ref=dsend.at[j], dst_ref=drecv.at[j],
+            send_sem=d_s.at[j], recv_sem=d_r.at[j],
             device_id={"tp": partner}, device_id_type=MESH,
         )
 
-    def x_copy(j):
-        return pltpu.make_async_remote_copy(
-            src_ref=xsend.at[j], dst_ref=xrecv.at[j],
-            send_sem=x_s.at[j], recv_sem=x_r.at[j],
-            device_id={"tp": across}, device_id_type=MESH,
-        )
-
-    def product(h, first_row, j):
-        cols = pl.ds(pl.multiple_of(j * cw, cw), cw)
-        w = ow[:, cols]
-        theirs = att[pl.ds(first_row + (1 - core) * quarter, quarter), :]
-        dsend[h, j] = jnp.dot(theirs, w, preferred_element_type=F32).astype(BF16)
-        d_copy(h, j).start()
-        ours = att[pl.ds(first_row + core * quarter, quarter), :]
-        mine[h, j] = jnp.dot(ours, w, preferred_element_type=F32).astype(BF16)
-
-    def forward(j):
-        d_copy(0, j).wait_recv()
-        xsend[j] = (mine[0, j].astype(F32) + drecv[0, j].astype(F32)).astype(BF16)
-        x_copy(j).start()
+    def e_copy(i):
+        return pltpu.make_async_remote_copy(
+            src_ref=esend.at[i], dst_ref=erecv.at[i],
+            send_sem=e_s.at[i], recv_sem=e_r.at[i],
+            device_id={"tp": partner}, device_id_type=MESH,
+        )
+
+    def x_copy(k):
+        step = lax.rem(k, half_blocks)
+        return pltpu.make_async_remote_copy(
+            src_ref=xsend.at[k], dst_ref=xrecv.at[core, step],
+            send_sem=x_s.at[k], recv_sem=x_r.at[core, step],
+            device_id={"tp": (1 - side) * 2 + k // half_blocks}, device_id_type=MESH,
+        )
+
+    def x_arrival(c, step):
+        return pltpu.make_async_remote_copy(
+            src_ref=xsend.at[step], dst_ref=xrecv.at[c, step],
+            send_sem=x_s.at[step], recv_sem=x_r.at[c, step],
+            device_id={"tp": (1 - side) * 2 + core}, device_id_type=MESH,
+        )
 
     other_first = (1 - side) * half_blocks
-    lax.fori_loop(other_first, other_first + half_blocks, attend, 0)
+
+    def early_block(i):
+        attend(other_first + i, 0)
+        a = att[pl.ds((other_first + i) * SB, SB), :]
+        for j in range(side_cols // cw):
+            cols = pl.ds(pl.multiple_of((1 - core) * side_cols + j * cw, cw), cw)
+            esend[i, :, j * cw : (j + 1) * cw] = jnp.dot(
+                a, ow[:, cols], preferred_element_type=F32
+            ).astype(BF16)
+        e_copy(i).start()
+        for j in range(side_cols // cw):
+            cols = pl.ds(pl.multiple_of(core * side_cols + j * cw, cw), cw)
+            early[i, :, j * cw : (j + 1) * cw] = jnp.dot(
+                a, ow[:, cols], preferred_element_type=F32
+            ).astype(BF16)
+
+    def forward(i):
+        e_copy(i).wait_recv()
+        for k in range(2):
+            r = slice(k * step_rows, (k + 1) * step_rows)
+            xsend[2 * i + k] = (early[i, r].astype(F32) + erecv[i, r].astype(F32)).astype(BF16)
+            x_copy(2 * i + k).start()
+
     load.wait()
-    product(0, other_first * SB, 0)
-
-    def first_step(j, carry):
-        product(0, other_first * SB, j)
-        forward(j - 1)
-        return carry
-
-    lax.fori_loop(1, chunks, first_step, 0)
-    forward(chunks - 1)
+
+    def early_step(i, carry):
+        early_block(i)
+        forward(i)
+        return carry
+
+    lax.fori_loop(0, half_blocks, early_step, 0)
 
     own_first = side * half_blocks
     lax.fori_loop(own_first, own_first + half_blocks, attend, 0)
 
-    def second_step(j, carry):
-        product(1, own_first * SB, j)
-        return carry
-
-    lax.fori_loop(0, chunks, second_step, 0)
-
-    def last_step(j, carry):
+    def own_step(j, carry):
+        w = ow[:, pl.ds(pl.multiple_of(j * cw, cw), cw)]
+        theirs = att[pl.ds(own_first * SB + (1 - core) * quarter, quarter), :]
+        dsend[j] = jnp.dot(theirs, w, preferred_element_type=F32).astype(BF16)
+        d_copy(j).start()
+        ours = att[pl.ds(own_first * SB + core * quarter, quarter), :]
+        mine[j] = jnp.dot(ours, w, preferred_element_type=F32).astype(BF16)
+        return carry
+
+    lax.fori_loop(0, chunks, own_step, 0)
+
+    def base_step(j, carry):
+        d_copy(j).wait_recv()
         cols = pl.ds(pl.multiple_of(j * cw, cw), cw)
-        d_copy(1, j).wait_recv()
-        x_copy(j).wait_recv()
-        total = mine[1, j].astype(F32) + drecv[1, j].astype(F32) + xrecv[j].astype(F32)
-        out_ref[:, cols] = total.astype(BF16)
-        d_copy(0, j).wait_send()
-        d_copy(1, j).wait_send()
-        x_copy(j).wait_send()
-        return carry
-
-    lax.fori_loop(0, chunks, last_step, 0)
+        base[:, cols] = mine[j].astype(F32) + drecv[j].astype(F32)
+        d_copy(j).wait_send()
+        return carry
+
+    lax.fori_loop(0, chunks, base_step, 0)
+
+    def last_step(k, carry):
+        r = pl.ds(pl.multiple_of(k * step_rows, step_rows), step_rows)
+        for c in range(2):
+            x_arrival(c, k).wait_recv()
+            cols = slice(c * side_cols, (c + 1) * side_cols)
+            out_ref[r, cols] = (base[r, cols] + xrecv[c, k].astype(F32)).astype(BF16)
+        e_copy(k).wait_send()
+        x_copy(k).wait_send()
+        x_copy(half_blocks + k).wait_send()
+        return carry
+
+    lax.fori_loop(0, half_blocks, last_step, 0)
 
 
 def local(
@@ -348,8 +427,6 @@
     summary_pos, key_mixing, value_mixing, out_weight, chosen,
 ):
     rows, depth = tokens.shape
-    me = lax.axis_index("kv")
-    tp = lax.axis_index("tp")
     heads = query_weight.shape[1] // HD
     G = key_weight.shape[1] // HD
     R = heads // G
@@ -363,40 +440,13 @@
     oc = width // cw
     gates_all = gate_weight.shape[1]
 
-    source = chosen // nb
-    inside = chosen - source * nb
-    hit = source[None] == jnp.arange(n, dtype=jnp.int32)[:, None, None, None]
-    lo = jnp.min(jnp.where(hit, inside[None], nb), axis=(1, 3))
-    hi = jnp.max(jnp.where(hit, inside[None], -1), axis=(1, 3))
-    lo = jnp.where(lo == nb, 0, lo)
-    hi = jnp.where(hi < 0, 0, hi)
-    req = jnp.stack([lo, hi], axis=-1).reshape(n, G * 2)
-    req = jnp.pad(req, ((0, 0), (0, 8 - G * 2)))
-    req = jnp.broadcast_to(req[:, :, None], (n, 8, LANES))
-    low_of = jnp.sum(jnp.where(hit, lo[:, None, :, None], 0), axis=0)
-    head = jnp.arange(G, dtype=jnp.int32)[None, :, None]
-    away = G * nb + (source * G + head) * 2 + (inside != low_of).astype(jnp.int32)
-    index = jnp.where(source == me, head * nb + inside, away).reshape(-1)
-    bias = jnp.where(first_named(chosen), 0.0, LOW)
-    bias = jnp.broadcast_to(bias[..., None], (nb, G, N_SEL, SB)).reshape(nb * G, 1, N_SEL * SB)
-
-    km = lax.dynamic_slice_in_dim(key_mixing, tp * G, G, 1).astype(F32).T
-    vm = lax.dynamic_slice_in_dim(value_mixing, tp * G, G, 1).astype(F32).T
-    mix = jnp.concatenate(
-        [
-            jnp.broadcast_to(km[:, :, None], (G, CMP, HD)),
-            jnp.broadcast_to(vm[:, :, None], (G, CMP, HD)),
-        ],
-        axis=-1,
-    )
-    pos = jnp.concatenate([summary_pos, summary_pos], axis=-1).astype(F32)
-
     vmem = pl.BlockSpec(memory_space=pltpu.VMEM)
     hbm = pl.BlockSpec(memory_space=pl.ANY)
     smem = pl.BlockSpec(memory_space=pltpu.SMEM)
     dma = pltpu.SemaphoreType.DMA
     table = G * nb + n * G * 2
-    queries, gates, tab, summary = pl.pallas_call(
+    nbp = -(-nb // 8) * 8
+    queries, gates, tab, summary, index, bias = pl.pallas_call(
         functools.partial(project_kernel, n, G, R, nb, kc, pad),
         name="project",
         out_shape=[
@@ -404,18 +454,23 @@
             jax.ShapeDtypeStruct((rows, gates_all), F32),
             jax.ShapeDtypeStruct((table, SB, LANES), BF16),
             jax.ShapeDtypeStruct((n, G, pad, LANES), BF16),
+            jax.ShapeDtypeStruct((G, nb, N_SEL), jnp.int32),
+            jax.ShapeDtypeStruct((G, nbp, N_SEL * SB), F32),
         ],
-        in_specs=[hbm] * 5 + [vmem] * 3,
-        out_specs=[vmem] * 4,
+        in_specs=[hbm] * 5 + [vmem] * 4,
+        out_specs=[vmem] * 6,
         scratch_shapes=[
             pltpu.VMEM((rows, depth), BF16),
             pltpu.VMEM((depth, heads * HD), BF16),
             pltpu.VMEM((depth, 2 * G * HD), BF16),
-            pltpu.VMEM((depth, gates_all), BF16),
+            pltpu.VMEM((gates_all, depth), BF16),
             pltpu.VMEM((rows, heads * HD), F32),
             pltpu.VMEM((rows, gates_all), F32),
             pltpu.VMEM((G, nb, SB, LANES), F32),
-            pltpu.VMEM((n, 8, LANES), jnp.int32),
+            pltpu.VMEM((nbp, LANES), F32),
+            pltpu.VMEM((CMP, LANES), F32),
+            pltpu.VMEM((n, 8, LANES), F32),
+            pltpu.VMEM((n, 8, LANES), F32),
             pltpu.VMEM((n, G * 2, SB, LANES), BF16),
             pltpu.VMEM((G, pad, LANES), BF16),
             dma((chunks,)), dma((chunks,)), dma((chunks,)), dma((chunks,)), dma((chunks,)),
@@ -424,9 +479,13 @@
         compiler_params=pltpu.CompilerParams(
             collective_id=1, has_side_effects=True, vmem_limit_bytes=VMEM_LIMIT
         ),
-    )(tokens, query_weight, key_weight, value_weight, gate_weight, req, mix, pos)
+    )(
+        tokens, query_weight, key_weight, value_weight, gate_weight.T,
+        chosen, key_mixing.T, value_mixing.T, summary_pos,
+    )
 
     quarter = rows // 4
+    half = nb // 2
     return pl.pallas_call(
         functools.partial(attend_kernel, n, G, R, nb, pad, spans, cw),
         name="attend",
@@ -437,12 +496,16 @@
             pltpu.VMEM(out_weight.shape, BF16),
             pltpu.VMEM((rows, heads * HD), BF16),
             pltpu.VMEM((G, N_SEL * SB, LANES), BF16),
-            pltpu.VMEM((2, oc, quarter, cw), BF16),
-            pltpu.VMEM((2, oc, quarter, cw), BF16),
-            pltpu.VMEM((2, oc, quarter, cw), BF16),
             pltpu.VMEM((oc, quarter, cw), BF16),
             pltpu.VMEM((oc, quarter, cw), BF16),
-            dma, dma((2, oc)), dma((2, oc)), dma((oc,)), dma((oc,)),
+            pltpu.VMEM((oc, quarter, cw), BF16),
+            pltpu.VMEM((half, SB, width // 2), BF16),
+            pltpu.VMEM((half, SB, width // 2), BF16),
+            pltpu.VMEM((half, SB, width // 2), BF16),
+            pltpu.VMEM((2 * half, SB // 2, width // 2), BF16),
+            pltpu.VMEM((2, half, SB // 2, width // 2), BF16),
+            pltpu.VMEM((quarter, width), F32),
+            dma, dma((oc,)), dma((oc,)), dma((half,)), dma((half,)), dma((2 * half,)), dma((2, half)),
         ],
         compiler_params=pltpu.CompilerParams(
             collective_id=2, has_side_effects=True, vmem_limit_bytes=VMEM_LIMIT

time: 83.3 us -> 66.3 us (0.80)
  other arithmetic: 5.96 us -> 0 us
  Pallas kernels: 69.2 us -> 63.6 us
  local copies, waits for them, and re-layouts: 7.31 us -> 2.49 us
    pallas_call x1, Pallas kernels: 46.1 us -> 40.4 us  [local(): pl.pallas_call(functools.partial(attend_kernel, n, G, R, nb, pad, spans,...]
    unnamed x3 -> x1, local copies, waits for them, and re-layouts: 4.93 us -> 2.49 us
    reshape x2 -> x0, local copies, waits for them, and re-layouts: 1.46 us -> none  [the longest x1 0.78 us: local(): jnp.broadcast_to(bias[..., None], (nb, G, N_SEL, SB))]
    convert_element_type x1 -> x0, other arithmetic: 1.45 us -> none  [local(): pos = jnp.concatenate([summary_pos, summary_pos], axis=-1).astype(F32)]
    reduce_or x1 -> x0, other arithmetic: 1.29 us -> none  [first_named(): return jnp.logical_not(jnp.any(repeated & earlier, axis=-1))]
    broadcast_in_dim x4 -> x0, local copies, waits for them, and re-layouts: 0.91 us -> none  [the longest x1 0.67 us: local(): req = jnp.broadcast_to(req[:, :, None], (n, 8, LANES))]
where the time goes in v2:
time: 66.3 us; the launch traced here: 66.1 us
  Pallas kernels  63.6 us (96%)
  local copies, waits for them, and re-layouts  2.49 us (4%)
    pallas_call x1, Pallas kernels, local(): pl.pallas_call(functools.partial(attend_kernel, n, G, R, nb, pad, spans,...  40.4 us
    pallas_call x1, Pallas kernels, local(): pl.pallas_call(functools.partial(project_kernel, n, G, R, nb, kc, pad), n...  23.2 us
    unnamed x1, local copies, waits for them, and re-layouts  2.49 us

profile of v2, /device:TPU:29, one launch (start us, length us, event | category | flops | bytes accessed | tf_op | source)
XLA Modules:
  0.0 66.1 jit_solution(3414195507941029816)
XLA Ops:
  0.0 23.2 %project.1 = (bf16[2,10,256,128]{3,2,1,0:T(8,128)(2,1)}, f32[640,64]{1,0:T(8,128)}, bf16[52,64,128]{2,1,0:T(8,128)(2,1)}, bf16[8,2,32,128]{3,2,1,0:T(8,128)(2,1)...) custom-call(bf16[640,4096]{1,0:T(8,128)(2,1)} %tok_hbm.1, bf16[4096,512]{1,0:T(8,128)(2,1)} %qw_hbm.1, ...), custom_call_target="tpu_custom_call" | custom-call | tf_op jit(solution)/shard_map/project/pallas_call | solution.py:449
  23.2 40.4 %attend.1 = bf16[160,4096]{1,0:T(8,128)(2,1)} custom-call(s32[2,10,16]{2,1,0:T(8,128)} %get-tuple-element.11.idx_ref, bf16[2,10,256,128]{3,2,1,0:T(8,128)(2,1)} %get-tuple-element.12.qp_ref, f32[640,64]{1,0:T(8,128)} %get-tuple-element.13.gate_ref, bf16[52,64,128]{2,1,0:T(8,128)(2,1)} %get-tuple-element.14.tab_ref, ...), custom_call_target="tpu_custom_call" | custom-call | tf_op jit(solution)/shard_map/attend/pallas_call | solution.py:489
  63.6 2.5 %copy.12 = bf16[160,4096]{1,0:T(8,128)(2,1)} copy(bf16[160,4096]{1,0:T(8,128)(2,1)} %attend.1) | data formatting | bytes 2621440

commit v3 on v2

--- a/solution.py
+++ b/solution.py
@@ -19,14 +19,15 @@
 VMEM_LIMIT = 64_000_000
 
 
-def project_kernel(
-    n, G, R, nb, kc, pad,
+def project(
+    n, G, R, nb, kc, pad, ow_load, idx_smem, sem_idx,
     tok_hbm, qw_hbm, kw_hbm, vw_hbm, gw_hbm, ch_ref, km_ref, vm_ref, pos_in,
     qp_ref, gate_ref, tab_ref, sum_ref, idx_ref, bias_ref,
-    tok, qw, kvw, gw, acc, gacc, tf, named, pos_ref, req_ref, req_in, send, sum_send,
+    tok, qw, kvw, gw, acc, gacc, tf, named, pos_ref, req_ref, req_in, req_smem, sem_req, send, sum_send,
     sem_tok, sem_kw, sem_vw, sem_qw, sem_gw,
     req_s, req_r, blk_s, blk_r, sum_s, sum_r,
 ):
+    tp = lax.axis_index("tp")
     me = lax.axis_index("kv")
     rows = nb * SB
     depth = tok.shape[1]
@@ -56,45 +57,50 @@
     for i in range(chunks):
         for c in late(i):
             c.start()
+    ow_load.start()
 
     barrier = pltpu.get_barrier_semaphore()
     for i in range(1, n):
         pl.semaphore_signal(
             barrier, inc=1, device_id={"kv": lax.rem(me + i, n)}, device_id_type=MESH
         )
+    for i in range(1, 4):
+        pl.semaphore_signal(barrier, inc=1, device_id={"tp": lax.rem(tp + i, 4)}, device_id_type=MESH)
 
     place = lax.broadcasted_iota(jnp.int32, named.shape, 1)
     slot_row = lax.broadcasted_iota(jnp.int32, (LANES, N_SEL * SB), 0)
     slot_col = lax.broadcasted_iota(jnp.int32, (LANES, N_SEL * SB), 1) // SB
     spread = jnp.where(slot_row == slot_col, 1.0, 0.0).astype(BF16)
     for g in range(G):
-        named[...] = jnp.full(named.shape, -1.0, F32)
-        named[:nb, :N_SEL] = ch_ref[:, g, :].astype(F32)
+        named[...] = jnp.full(named.shape, -1, jnp.int32)
+        named[:nb, :N_SEL] = ch_ref[:, g, :]
         c = named[...]
         source = jnp.zeros_like(c)
         for s in range(1, n):
-            source = source + jnp.where(c >= s * nb, 1.0, 0.0)
+            source = source + jnp.where(c >= s * nb, 1, 0)
         inside = c - source * nb
         low_of = jnp.zeros_like(c)
         for s in range(n):
-            hit = (c >= 0.0) & (source == s)
-            lo = jnp.where(hit, inside, float(nb))
+            hit = (c >= 0) & (source == s)
+            lo = jnp.where(hit, inside, nb)
             lo = jnp.min(jnp.min(lo, axis=0, keepdims=True), axis=1, keepdims=True)
-            lo = jnp.where(lo == nb, 0.0, lo)
-            hi = jnp.where(hit, inside, 0.0)
+            lo = jnp.where(lo == nb, 0, lo)
+            hi = jnp.where(hit, inside, 0)
             hi = jnp.max(jnp.max(hi, axis=0, keepdims=True), axis=1, keepdims=True)
             low_of = jnp.where(hit, lo, low_of)
             req_ref[s, 2 * g : 2 * g + 1] = jnp.broadcast_to(lo, (1, LANES))
             req_ref[s, 2 * g + 1 : 2 * g + 2] = jnp.broadcast_to(hi, (1, LANES))
-        away = G * nb + (source * G + g) * 2 + jnp.where(inside != low_of, 1.0, 0.0)
-        at = jnp.where(source == me.astype(F32), g * nb + inside, away)
-        idx_ref[g] = at[:nb, :N_SEL].astype(jnp.int32)
-        again = jnp.zeros_like(c)
+        away = G * nb + (source * G + g) * 2 + jnp.where(inside != low_of, 1, 0)
+        at = jnp.where(source == me, g * nb + inside, away)
+        idx_ref[g] = jnp.where(c >= 0, at, 0)
+        again = jnp.zeros(c.shape, F32)
         for d in range(1, N_SEL):
             again = jnp.where((place >= d) & (pltpu.roll(c, d, 1) == c), 1.0, again)
         bias_ref[g] = jnp.dot(again.astype(BF16), spread, preferred_element_type=F32) * LOW
 
-    pl.semaphore_wait(barrier, n - 1)
+    idx_copy = pltpu.make_async_copy(idx_ref, idx_smem, sem_idx)
+    idx_copy.start()
+    pl.semaphore_wait(barrier, n + 2)
 
     def req_copy(i):
         return pltpu.make_async_remote_copy(
@@ -157,7 +163,7 @@
             first = jnp.where(lower, keys, pltpu.roll(vals, HD, 1))
             second = jnp.where(lower, pltpu.roll(keys, HD, 1), vals)
             for g, t in ((2 * pair, first), (2 * pair + 1, second)):
-                tf[g, b] = t
+                tf[g * nb + b] = t.astype(BF16)
                 tab_ref[g * nb + b] = t.astype(BF16)
         return carry
 
@@ -180,7 +186,7 @@
         km = mix_column(km_ref, head)
         vm = mix_column(vm_ref, head)
         mix = jnp.where(mix_low, km, vm)
-        t = tf[g].reshape(spans, CMP, LANES)
+        t = tf[g * nb : (g + 1) * nb].astype(F32).reshape(spans, CMP, LANES)
         w = (t + pos_ref[...][None]) * mix[None]
         s = jnp.sum(w, axis=1)
         s = jnp.concatenate([s, jnp.zeros((pad - spans, LANES), F32)], axis=0)
@@ -190,17 +196,14 @@
         sum_copy(i).start()
     for i in range(1, n):
         req_copy(i).wait_recv()
+        pltpu.make_async_copy(req_in.at[i], req_smem.at[i], sem_req.at[i]).start()
+    for i in range(1, n):
+        pltpu.make_async_copy(req_in.at[i], req_smem.at[i], sem_req.at[i]).wait()
 
         @pl.when(me + i < n)
         def _():
-            wanted = req_in[i]
             for k in range(G * 2):
-                g = k // 2
-                want = jnp.broadcast_to(wanted[k : k + 1], (SB, LANES))
-                block = tf[g, 0]
-                for b in range(1, nb):
-                    block = jnp.where(want == float(b), tf[g, b], block)
-                send[i, k] = block.astype(BF16)
+                send[i, k] = tf[(k // 2) * nb + req_smem[i, k, 0]]
             blk_copy(i).start()
 
     acc[...] = jnp.zeros_like(acc)
@@ -231,6 +234,7 @@
         return carry
 
     lax.fori_loop(0, nb, query_step, 0)
+    idx_copy.wait()
     for i in range(1, n):
         sum_arrival(i).wait_recv()
         sum_copy(i).wait_send()
@@ -245,12 +249,12 @@
             blk_arrival(i).wait_recv()
 
 
-def attend_kernel(
-    n, G, R, nb, pad, spans, cw,
-    idx_ref, qp_ref, gate_ref, tab_ref, sum_ref, bias_ref, ow_hbm,
+def attend_and_mix(
+    n, G, R, nb, pad, spans, cw, load,
+    idx_ref, qp_ref, gate_ref, tab_ref, sum_ref, bias_ref,
     out_ref,
     ow, att, kbuf, mine, dsend, drecv, early, esend, erecv, xsend, xrecv, base,
-    sem_w, d_s, d_r, e_s, e_r, x_s, x_r,
+    d_s, d_r, e_s, e_r, x_s, x_r,
 ):
     me = lax.axis_index("kv")
     tp = lax.axis_index("tp")
@@ -265,14 +269,6 @@
     group_rows = R * SB
     side_cols = width // 2
     step_rows = SB // 2
-
-    load = pltpu.make_async_copy(ow_hbm, ow, sem_w)
-    load.start()
-
-    barrier = pltpu.get_barrier_semaphore()
-    for i in range(1, 4):
-        pl.semaphore_signal(barrier, inc=1, device_id={"tp": lax.rem(tp + i, 4)}, device_id_type=MESH)
-    pl.semaphore_wait(barrier, 3)
 
     row = lax.broadcasted_iota(jnp.int32, (group_rows, LANES), 0) % SB
     lane = lax.broadcasted_iota(jnp.int32, (group_rows, LANES), 1)
@@ -421,6 +417,22 @@
     lax.fori_loop(0, half_blocks, last_step, 0)
 
 
+def layer_kernel(n, G, R, nb, kc, pad, cw, *refs):
+    inputs, ow_hbm, out_ref = refs[:9], refs[9], refs[10]
+    qp, gate, tab, summary, idx, bias = refs[11:17]
+    idx_smem, sem_idx, ow, sem_w = refs[17:21]
+    first, second = refs[21 : 21 + 26], refs[21 + 26 :]
+    load = pltpu.make_async_copy(ow_hbm, ow, sem_w)
+    project(
+        n, G, R, nb, kc, pad, load, idx_smem, sem_idx,
+        *inputs, qp, gate, tab, summary, idx, bias, *first,
+    )
+    attend_and_mix(
+        n, G, R, nb, pad, nb * SB // CMP, cw, load,
+        idx_smem, qp, gate, tab, summary, bias, out_ref, ow, *second,
+    )
+
+
 def local(
     n,
     tokens, query_weight, key_weight, value_weight, gate_weight,
@@ -442,75 +454,71 @@
 
     vmem = pl.BlockSpec(memory_space=pltpu.VMEM)
     hbm = pl.BlockSpec(memory_space=pl.ANY)
-    smem = pl.BlockSpec(memory_space=pltpu.SMEM)
     dma = pltpu.SemaphoreType.DMA
     table = G * nb + n * G * 2
     nbp = -(-nb // 8) * 8
-    queries, gates, tab, summary, index, bias = pl.pallas_call(
-        functools.partial(project_kernel, n, G, R, nb, kc, pad),
-        name="project",
-        out_shape=[
-            jax.ShapeDtypeStruct((G, nb, R * SB, LANES), BF16),
-            jax.ShapeDtypeStruct((rows, gates_all), F32),
-            jax.ShapeDtypeStruct((table, SB, LANES), BF16),
-            jax.ShapeDtypeStruct((n, G, pad, LANES), BF16),
-            jax.ShapeDtypeStruct((G, nb, N_SEL), jnp.int32),
-            jax.ShapeDtypeStruct((G, nbp, N_SEL * SB), F32),
-        ],
-        in_specs=[hbm] * 5 + [vmem] * 4,
-        out_specs=[vmem] * 6,
+    quarter = rows // 4
+    half = nb // 2
+    stage_one = [
+        pltpu.VMEM((rows, depth), BF16),
+        pltpu.VMEM((depth, heads * HD), BF16),
+        pltpu.VMEM((depth, 2 * G * HD), BF16),
+        pltpu.VMEM((gates_all, depth), BF16),
+        pltpu.VMEM((rows, heads * HD), F32),
+        pltpu.VMEM((rows, gates_all), F32),
+        pltpu.VMEM((G * nb, SB, LANES), BF16),
+        pltpu.VMEM((nbp, LANES), jnp.int32),
+        pltpu.VMEM((CMP, LANES), F32),
+        pltpu.VMEM((n, 8, LANES), jnp.int32),
+        pltpu.VMEM((n, 8, LANES), jnp.int32),
+        pltpu.SMEM((n, 8, LANES), jnp.int32),
+        dma((n,)),
+        pltpu.VMEM((n, G * 2, SB, LANES), BF16),
+        pltpu.VMEM((G, pad, LANES), BF16),
+        dma((chunks,)), dma((chunks,)), dma((chunks,)), dma((chunks,)), dma((chunks,)),
+        dma((n,)), dma((n,)), dma((n,)), dma((n,)), dma((n,)), dma((n,)),
+    ]
+    stage_two = [
+        pltpu.VMEM((rows, heads * HD), BF16),
+        pltpu.VMEM((G, N_SEL * SB, LANES), BF16),
+        pltpu.VMEM((oc, quarter, cw), BF16),
+        pltpu.VMEM((oc, quarter, cw), BF16),
+        pltpu.VMEM((oc, quarter, cw), BF16),
+        pltpu.VMEM((half, SB, width // 2), BF16),
+        pltpu.VMEM((half, SB, width // 2), BF16),
+        pltpu.VMEM((half, SB, width // 2), BF16),
+        pltpu.VMEM((2 * half, SB // 2, width // 2), BF16),
+        pltpu.VMEM((2, half, SB // 2, width // 2), BF16),
+        pltpu.VMEM((quarter, width), F32),
+        dma((oc,)), dma((oc,)), dma((half,)), dma((half,)), dma((2 * half,)), dma((2, half)),
+    ]
+    return pl.pallas_call(
+        functools.partial(layer_kernel, n, G, R, nb, kc, pad, cw),
+        name="layer",
+        out_shape=jax.ShapeDtypeStruct((quarter, width), BF16),
+        in_specs=[hbm] * 5 + [vmem] * 4 + [hbm],
+        out_specs=vmem,
         scratch_shapes=[
-            pltpu.VMEM((rows, depth), BF16),
-            pltpu.VMEM((depth, heads * HD), BF16),
-            pltpu.VMEM((depth, 2 * G * HD), BF16),
-            pltpu.VMEM((gates_all, depth), BF16),
-            pltpu.VMEM((rows, heads * HD), F32),
+            pltpu.VMEM((G, nb, R * SB, LANES), BF16),
             pltpu.VMEM((rows, gates_all), F32),
-            pltpu.VMEM((G, nb, SB, LANES), F32),
-            pltpu.VMEM((nbp, LANES), F32),
-            pltpu.VMEM((CMP, LANES), F32),
-            pltpu.VMEM((n, 8, LANES), F32),
-            pltpu.VMEM((n, 8, LANES), F32),
-            pltpu.VMEM((n, G * 2, SB, LANES), BF16),
-            pltpu.VMEM((G, pad, LANES), BF16),
-            dma((chunks,)), dma((chunks,)), dma((chunks,)), dma((chunks,)), dma((chunks,)),
-            dma((n,)), dma((n,)), dma((n,)), dma((n,)), dma((n,)), dma((n,)),
+            pltpu.VMEM((table, SB, LANES), BF16),
+            pltpu.VMEM((n, G, pad, LANES), BF16),
+            pltpu.VMEM((G, nbp, LANES), jnp.int32),
+            pltpu.VMEM((G, nbp, N_SEL * SB), F32),
+            pltpu.SMEM((G, nbp, LANES), jnp.int32),
+            dma,
+            pltpu.VMEM(out_weight.shape, BF16),
+            dma,
+            *stage_one,
+            *stage_two,
         ],
         compiler_params=pltpu.CompilerParams(
             collective_id=1, has_side_effects=True, vmem_limit_bytes=VMEM_LIMIT
         ),
     )(
         tokens, query_weight, key_weight, value_weight, gate_weight.T,
-        chosen, key_mixing.T, value_mixing.T, summary_pos,
+        chosen, key_mixing.T, value_mixing.T, summary_pos, out_weight,
     )
-
-    quarter = rows // 4
-    half = nb // 2
-    return pl.pallas_call(
-        functools.partial(attend_kernel, n, G, R, nb, pad, spans, cw),
-        name="attend",
-        out_shape=jax.ShapeDtypeStruct((quarter, width), BF16),
-        in_specs=[smem] + [vmem] * 5 + [hbm],
-        out_specs=vmem,
-        scratch_shapes=[
-            pltpu.VMEM(out_weight.shape, BF16),
-            pltpu.VMEM((rows, heads * HD), BF16),
-            pltpu.VMEM((G, N_SEL * SB, LANES), BF16),
-            pltpu.VMEM((oc, quarter, cw), BF16),
-            pltpu.VMEM((oc, quarter, cw), BF16),
-            pltpu.VMEM((oc, quarter, cw), BF16),
-            pltpu.VMEM((half, SB, width // 2), BF16),
-            pltpu.VMEM((half, SB, width // 2), BF16),
-            pltpu.VMEM((half, SB, width // 2), BF16),
-            pltpu.VMEM((2 * half, SB // 2, width // 2), BF16),
-            pltpu.VMEM((2, half, SB // 2, width // 2), BF16),
-            pltpu.VMEM((quarter, width), F32),
-            dma, dma((oc,)), dma((oc,)), dma((half,)), dma((half,)), dma((2 * half,)), dma((2, half)),
-        ],
-        compiler_params=pltpu.CompilerParams(
-            collective_id=2, has_side_effects=True, vmem_limit_bytes=VMEM_LIMIT
-        ),
-    )(index, queries, gates, tab, summary, bias, out_weight)
 
 
 def solution(mesh):

time: 66.3 us -> 60.9 us (0.919)
  Pallas kernels: 63.6 us -> 58.2 us
    pallas_call x2 -> x1, Pallas kernels: 63.6 us -> 58.2 us  [local(): pl.pallas_call(functools.partial(layer_kernel, n, G, R, nb, kc, pad, cw),...]
where the time goes in v3:
time: 60.9 us; the launch traced here: 60.7 us
  Pallas kernels  58.2 us (96%)
  local copies, waits for them, and re-layouts  2.49 us (4%)
    pallas_call x1, Pallas kernels, local(): pl.pallas_call(functools.partial(layer_kernel, n, G, R, nb, kc, pad, cw),...  58.2 us
    unnamed x1, local copies, waits for them, and re-layouts  2.49 us

profile of v3, /device:TPU:29, one launch (start us, length us, event | category | flops | bytes accessed | tf_op | source)
XLA Modules:
  0.0 60.7 jit_solution(16963935084100962047)
XLA Ops:
  0.0 58.2 %layer.1 = bf16[160,4096]{1,0:T(8,128)(2,1)} custom-call(bf16[640,4096]{1,0:T(8,128)(2,1)} %refs_0_.1, bf16[4096,512]{1,0:T(8,128)(2,1)} %refs_1_.1, bf16[4096,128]{1,0:T(8,128)(2,1)} %refs_2_.1, bf16[4096,128]{1,0:T(8,128)(2,1)} %refs_3_.1, bf16[64,4096]{1,0:T(8,128)(2,1)} %bitcast.3, s32[10,2,16]{2,1,0:T(2,128)} %refs_5_.1, bf16[8,32]{1,0:T(8,128)(2,1)} %bitcast.4, ...), custom_call_target="tpu_custom_call" | custom-call | tf_op jit(solution)/shard_map/layer/pallas_call | solution.py:495
  58.2 2.5 %copy.12 = bf16[160,4096]{1,0:T(8,128)(2,1)} copy(bf16[160,4096]{1,0:T(8,128)(2,1)} %layer.1) | data formatting | bytes 2621440
